TPU v7x, 512 devices: a whole 4x8x8 slice. The times are simulated.
512 devices in a mesh: sp: 32 (over z, x), tp: 16 (over y, core).
Axes of the slice: x: 4, y: 8, z: 8, core: 2. Of those that a mesh axis runs over, the one named last changes fastest.
Arguments:
- moe_input: bfloat16 [6144, 2048], P('sp'), may hold values from -6 to 6
- out_grad: bfloat16 [6144, 2048], P('sp', 'tp'), may hold values from -6 to 6
- expert_ids: int32 [6144, 2], P('sp'), may hold values from 0 to 31, all different within a row; in each aligned block of 192 rows (0 to 191, 192 to 383, ...) at most 15 rows name the same one
- expert_weights: float32 [6144, 2], P('sp'), may hold values from 0.1 to 0.9
- w_gate: bfloat16 [32, 2048, 2048], P('sp', None, 'tp'), may hold values from -0.125 to 0.125
- w_up: bfloat16 [32, 2048, 2048], P('sp', None, 'tp'), may hold values from -0.125 to 0.125
- w_down: bfloat16 [32, 2048, 2048], P('sp', 'tp'), may hold values from -0.125 to 0.125
- out_proj: bfloat16 [1536, 2048], P('tp'), may hold values from -0.15625 to 0.15625
- retained: bfloat16 [6144, 1536], P('sp', 'tp'), may hold values from -6 to 6
- queries: bfloat16 [6144, 768], P('sp', 'tp'), may hold values from -6 to 6
- keys: bfloat16 [6144, 768], P('sp', 'tp'), may hold values from -0.86328125 to 0.86328125
- values: bfloat16 [6144, 1536], P('sp', 'tp'), may hold values from -6 to 6
- log_decay: float32 [6144, 16], P('sp', 'tp'), may hold values from -1 to 0
- incoming_state: float32 [32, 16, 48, 96], P('sp', 'tp'), may hold values from -6 to 6
Outputs:
- w_gate_grad: bfloat16 [32, 2048, 2048], P('sp', None, 'tp')
- w_up_grad: bfloat16 [32, 2048, 2048], P('sp', None, 'tp')
- w_down_grad: bfloat16 [32, 2048, 2048], P('sp', 'tp')
- out_proj_grad: float32 [2048, 1536], P('sp', 'tp')
- query_grad: bfloat16 [6144, 768], P('sp', 'tp')
- key_grad: bfloat16 [6144, 768], P('sp', 'tp')
- value_grad: bfloat16 [6144, 1536], P('sp', 'tp')
Inputs may be any that keep to these rules, and one draw needn't show every extreme that they name: `expert_ids`: in each aligned block of 192 positions no expert is named by more than 15 of the block's assignments, a bound that some block reaches.
All inputs are finite; a program needn't handle non-finite values.
Results may differ from a plain program's by a relative error of at most 0.02.
Values may be sent and summed in bfloat16 or wider, within the bound.
No kernel may reach another device: no remote copies, remote signals or barrier semaphores. Data moves between devices by JAX's collectives and lax.ppermute only.
A program may use at most 64 MiB of HBM per device.

v0:
```python
import jax
import jax.numpy as jnp
from jax import lax
from jax.sharding import Mesh
from jax.sharding import PartitionSpec as P

TP = ("y", "c")
F32 = jnp.float32
BF16 = jnp.bfloat16
ACROSS = (((1,), (1,)), ((), ()))
ALONG = (((0,), (0,)), ((), ()))
SWAP = [(0, 1), (1, 0)]


def dot(a, b, dims=(((1,), (0,)), ((), ()))):
    return lax.dot_general(a, b, dims, preferred_element_type=F32)


def slot_tables(expert_ids, expert_weights, experts, capacity, padded):
    tokens = expert_ids.shape[0]
    ids = expert_ids.T
    weights = expert_weights.T
    names = jnp.arange(experts, dtype=jnp.int32)[:, None]
    onehot = [(names == ids[j][None, :]).astype(BF16) for j in (0, 1)]
    place = jnp.arange(tokens)
    earlier = (place[:, None] < place[None, :]).astype(BF16)
    before = dot(onehot[0] + onehot[1], earlier)
    slots = jnp.arange(experts * padded, dtype=jnp.int32)[:, None]
    picker, slot_weight = (0.0, 0.0)
    for j in (0, 1):
        rank = jnp.sum(before * onehot[j].astype(F32), axis=0).astype(jnp.int32)
        hits = slots == (ids[j] * padded + rank)[None, :]
        picker = picker + jnp.where(hits, 1.0, 0.0)
        slot_weight = slot_weight + jnp.sum(
            jnp.where(hits, weights[j][None, :], 0.0), axis=1, keepdims=True
        )
    return (picker.astype(BF16), slot_weight)


def parity_columns(x, index):
    rows, cols = x.shape
    return lax.dynamic_index_in_dim(
        x.reshape(rows, 8, 2, cols // 16), index, 2, keepdims=False
    ).reshape(rows, cols // 2)


def parity_rows(x, index):
    rows, cols = x.shape
    return lax.dynamic_index_in_dim(
        x.reshape(8, 2, rows // 16, cols), index, 1, keepdims=False
    ).reshape(rows // 2, cols)


def joined_rows(own, other, core):
    rows, cols = own.shape
    own, other = (a.reshape(8, 1, rows // 8, cols) for a in (own, other))
    first = jnp.where(core == 0, own, other)
    second = jnp.where(core == 0, other, own)
    return jnp.concatenate([first, second], axis=1).reshape(2 * rows, cols)


def joined_columns(own, other, core):
    rows, cols = own.shape
    own, other = (a.reshape(rows, 8, 1, cols // 8) for a in (own, other))
    first = jnp.where(core == 0, own, other)
    second = jnp.where(core == 0, other, own)
    return jnp.concatenate([first, second], axis=2).reshape(rows, 2 * cols)


def in_three(x):
    high = x.astype(BF16)
    rest = x - high.astype(F32)
    middle = rest.astype(BF16)
    low = (rest - middle.astype(F32)).astype(BF16)
    return (high, middle, low)


def on_device(
    moe_input,
    out_grad,
    expert_ids,
    expert_weights,
    w_gate,
    w_up,
    w_down,
    out_proj,
    retained,
    queries,
    keys,
    values,
    log_decay,
    incoming_state,
):
    tokens = moe_input.shape[0]
    width = moe_input.shape[1]
    sp_count = lax.axis_size("sp")
    capacity = 5 * tokens // (2 * sp_count)
    padded = 16
    slot_count = sp_count * capacity
    core = lax.axis_index("c")
    block = lax.axis_index("sp")
    chunk = out_grad.shape[1]
    running = jnp.cumsum(log_decay[:, 0])
    last = running[-1]
    picker, slot_weight = slot_tables(expert_ids, expert_weights, sp_count, capacity, padded)
    mine = parity_columns(moe_input, core)
    send_rows = dot(picker, mine).astype(BF16).reshape(sp_count, padded, -1)
    parts = in_three(last)
    lane = jnp.arange(chunk)[None, None, :]
    extra = jnp.where(
        lane == 0, parts[0], jnp.where(lane == 1, parts[1], jnp.where(lane == 2, parts[2], 0.0))
    ).astype(BF16)
    send_grad = (dot(picker, out_grad) * slot_weight).astype(BF16).reshape(sp_count, padded, -1)
    spot = jnp.arange(padded)[None, :, None]
    send_grad = jnp.where(spot == padded - 1, extra, send_grad)
    got_grad = lax.all_to_all(send_grad, "sp", 0, 0, tiled=True)
    got_rows = lax.all_to_all(send_rows, "sp", 0, 0, tiled=True)
    rows_own = got_rows[:, :capacity].reshape(slot_count, -1)
    grad_part = got_grad[:, :capacity].reshape(slot_count, -1)
    ends = jnp.sum(got_grad[:, capacity, :3].astype(F32), axis=1)
    grad_own = lax.all_gather(grad_part, "y", axis=1, tiled=True)
    rows_other = lax.ppermute(rows_own, "c", SWAP)
    grad_other = lax.ppermute(grad_own, "c", SWAP)
    gate_own, gate_other = (parity_rows(w_gate[0], k) for k in (core, 1 - core))
    up_own, up_other = (parity_rows(w_up[0], k) for k in (core, 1 - core))
    down_own, down_other = (parity_columns(w_down[0], k) for k in (core, 1 - core))
    gate = dot(rows_own, gate_own) + dot(rows_other, gate_other)
    up = dot(rows_own, up_own) + dot(rows_other, up_other)
    sig = jax.nn.sigmoid(gate)
    swish = gate * sig
    act = (swish * up).astype(BF16)
    act_grad = dot(grad_own, down_own, ACROSS) + dot(grad_other, down_other, ACROSS)
    gate_grad = (act_grad * up * sig * (1.0 + gate * (1.0 - sig))).astype(BF16)
    up_grad = (act_grad * swish).astype(BF16)
    partial_other = (dot(gate_grad, gate_other, ACROSS) + dot(up_grad, up_other, ACROSS)).astype(
        BF16
    )
    arrived = lax.ppermute(partial_other, "c", SWAP)
    partial_own = dot(gate_grad, gate_own, ACROSS) + dot(up_grad, up_own, ACROSS)
    pair = (partial_own + arrived.astype(F32)).astype(BF16)
    pieces = jnp.moveaxis(pair.reshape(slot_count, 8, chunk), 1, 0)
    pieces = lax.all_to_all(pieces, "y", 0, 0, tiled=True)
    share = jnp.sum(pieces.astype(F32), axis=0).astype(BF16)
    gate_w_grad = joined_rows(
        dot(rows_own, gate_grad, ALONG).astype(BF16),
        dot(rows_other, gate_grad, ALONG).astype(BF16),
        core,
    )
    up_w_grad = joined_rows(
        dot(rows_own, up_grad, ALONG).astype(BF16),
        dot(rows_other, up_grad, ALONG).astype(BF16),
        core,
    )
    down_grad = joined_columns(
        dot(act, grad_own, ALONG).astype(BF16), dot(act, grad_other, ALONG).astype(BF16), core
    )
    returned = lax.all_to_all(share.reshape(sp_count, capacity, chunk), "sp", 0, 0, tiled=True)
    returned = jnp.pad(returned, ((0, 0), (0, padded - capacity), (0, 0)))
    token_grad = dot(picker, returned.reshape(sp_count * padded, chunk), ALONG)
    stream_part = (out_grad.astype(F32) + token_grad).astype(BF16)
    stream = lax.all_gather(stream_part, TP, axis=1, tiled=True)
    ret_grad = dot(stream, out_proj, ACROSS).astype(BF16)
    q, k, v, o = (a.astype(F32) for a in (queries, keys, values, ret_grad))
    rising = jnp.exp(running)[:, None]
    inject = dot(q * rising, o, ALONG)
    value_dim = values.shape[1]
    sent = jnp.broadcast_to(inject.astype(BF16)[None], (sp_count, *inject.shape))
    states = lax.all_to_all(sent, "sp", 0, 0, tiled=True)
    proj_part = dot(stream, retained, ALONG).astype(BF16)
    proj_parts = lax.all_to_all(
        proj_part.reshape(sp_count, width // sp_count, value_dim), "sp", 0, 0, tiled=True
    )
    out_proj_grad = jnp.sum(proj_parts.astype(F32), axis=0)
    order = jnp.arange(sp_count)
    between = (order[None, :] > block) & (order[None, :] < order[:, None])
    factors = jnp.where(
        order > block, jnp.exp(jnp.sum(jnp.where(between, ends[None, :], 0.0), axis=1)), 0.0
    )
    state_grad = jnp.sum(factors[:, None, None] * states.astype(F32), axis=0)
    place = jnp.arange(tokens)
    causal = place[:, None] >= place[None, :]
    diff = running[:, None] - running[None, :]
    decay = jnp.where(causal, jnp.exp(jnp.minimum(diff, 0.0)), 0.0)
    scores = dot(q, k, ACROSS) * decay
    prob_grad = dot(o, v, ACROSS) * decay
    tail = jnp.exp(last - running)[:, None]
    query_grad = dot(prob_grad, k) + rising * dot(o, incoming_state[0, 0], ACROSS)
    key_grad = dot(prob_grad, q, ALONG) + tail * dot(v, state_grad, ACROSS)
    value_grad = dot(scores, o, ALONG) + tail * dot(k, state_grad)
    return (
        gate_w_grad[None],
        up_w_grad[None],
        down_grad[None],
        out_proj_grad,
        query_grad.astype(BF16),
        key_grad.astype(BF16),
        value_grad.astype(BF16),
    )


def solution(mesh):
    torus = Mesh(mesh.devices.reshape(mesh.shape["sp"], 8, 2), ("sp", "y", "c"))
    placed = (
        P("sp", None),
        P("sp", TP),
        P("sp", None),
        P("sp", None),
        P("sp", None, TP),
        P("sp", None, TP),
        P("sp", TP, None),
        P(TP, None),
        P("sp", TP),
        P("sp", TP),
        P("sp", TP),
        P("sp", TP),
        P("sp", TP),
        P("sp", TP, None, None),
    )
    return jax.shard_map(
        on_device,
        mesh=torus,
        in_specs=placed,
        out_specs=(
            P("sp", None, TP),
            P("sp", None, TP),
            P("sp", TP, None),
            P("sp", TP),
            P("sp", TP),
            P("sp", TP),
            P("sp", TP),
        ),
        check_vma=False,
    )
```

profile of v0, /device:TPU:2, one launch (start us, length us, event | category | flops | bytes accessed | tf_op | source)
XLA Modules:
  0.0 204.9 jit_solution(3928460115457227741)
XLA Ops:
  0.7 0.8 pad_bitcast_fusion
  4.0 0.8 fusion.40
  4.9 0.8 fusion.39
  5.7 0.8 multiply_add_fusion.1
  6.6 1.2 fusion.1
  7.8 0.7 broadcast_select_fusion.4
  8.6 13.5 %all-to-all-start.1 = ((bf16[32,16,128]{2,1,0:T(8,128)(2,1)}), bf16[32,16,128]{2,1,0:T(8,128)(2,1)S(1)}, u32[]{:S(2)}, u32[]{:S(2)}) async-start(bf16[32,16,128]{2,1,0:T(8,128)(2,1)} %broadcast_select_fusion.4), calls=%async_computation.1 | async-start | bytes 262144 | tf_op jit(solution)/shard_map/all_to_all | solution.py:116
  22.6 2.3 %dynamic-slice_reduce_fusion = bf16[192,8,128]{2,1,0:T(8,128)(2,1)S(1)} fusion(bf16[192,8,2,128]{3,2,1,0:T(2,128)(2,1)S(1)} %reshape.287, s32[]{:T(128)S(6)} %select_n.175), kind=kLoop, calls=%fused_computation.37 | loop fusion | bytes 786436 | tf_op jit(solution)/shard_map/jit(dynamic_index_in_dim)/dynamic_slice | solution.py:42
  25.0 1.6 convolution_convert_fusion.1
  26.6 4.3 %all-to-all-done.1 = bf16[32,16,128]{2,1,0:T(8,128)(2,1)S(1)} async-done(((bf16[32,16,128]{2,1,0:T(8,128)(2,1)}), bf16[32,16,128]{2,1,0:T(8,128)(2,1)S(1)}, u32[]{:S(2)}, u32[]{:S(2)}) %all-to-all-start.1) | async-done | bytes 131104 | tf_op jit(solution)/shard_map/all_to_all | solution.py:116
  30.9 5.5 %all-to-all-start = ((bf16[32,16,1024]{2,1,0:T(8,128)(2,1)}), bf16[32,16,1024]{2,1,0:T(8,128)(2,1)S(1)}, u32[]{:S(2)}, u32[]{:S(2)}) async-start(bf16[32,16,1024]{2,1,0:T(8,128)(2,1)} %bitcast.7), calls=%async_computation | async-start | bytes 2097152 | tf_op jit(solution)/shard_map/all_to_all | solution.py:117
  36.4 28.7 %all_gather.6 = bf16[480,1024]{1,0:T(8,128)(2,1)S(1)} all-gather(bf16[480,128]{1,0:T(8,128)(2,1)S(1)} %reshape.294), channel_id=1, replica_groups=mesh['sp'=32,'y'=8,'c'=2] {'y'}, dimensions={1}, use_global_device_ids=true | all-gather | bytes 1105920 | tf_op jit(solution)/shard_map/all_gather | solution.py:121
  65.1 1.9 collective-permute-start
  67.0 1.3 copy.47
  68.3 0.8 constant_dynamic-slice_fusion.4
  69.2 2.2 %constant_dynamic-slice_fusion = (bf16[8,1,128,128]{3,2,1,0:T(8,128)(2,1)}, bf16[8,1,128,128]{3,2,1,0:T(8,128)(2,1)}, bf16[8,1,128,128]{3,2,1,0:T(8,128)(2,1)}, bf16[8,1,128,128]{3,2,1,0:T(8,128)(2,1)}) fusion(bf16[8,2,128,128]{3,2,1,0:T(8,128)(2,1)} %bitcast.158, s32[]{:T(128)S(6)} %select_n.182, s32[]{:T(128)S(6)} %select_n.175, ...), kind=kLoop, calls=%fused_computation.88 | loop fusion | bytes 2097160 | tf_op jit(solution)/shard_map/jit(dynamic_index_in_dim)/dynamic_slice | solution.py:49
  71.7 2.5 %collective-permute-start.1 = (bf16[480,1024]{1,0:T(8,128)(2,1)S(1)}, bf16[480,1024]{1,0:T(8,128)(2,1)S(1)}, u32[]{:S(2)}, u32[]{:S(2)}) collective-permute-start(bf16[480,1024]{1,0:T(8,128)(2,1)S(1)} %reshape.290), channel_id=1, source_target_pairs={{0,1},{1,0},{2,3},{3,2},{4,5},{5,4},{6,7},{7,6},{8,9},{9,8},{10,11... | collective-permute-start | bytes 2949128 | tf_op jit(solution)/shard_map/ppermute | solution.py:122
  74.2 1.4 fusion.43
  75.6 1.7 convolution_add_fusion.2
  78.7 1.1 multiply_convert_fusion
  80.2 1.4 add_convert_fusion.1
  81.6 1.9 collective-permute-start.2
  84.3 1.2 fusion.27
  85.6 1.4 fusion.46
  87.0 1.6 fusion
  88.6 1.1 copy.65
  89.7 4.4 %all-to-all-start.2 = ((bf16[8,480,128]{2,1,0:T(8,128)(2,1)}), bf16[8,480,128]{2,1,0:T(8,128)(2,1)}, u32[]{:S(2)}, u32[]{:S(2)}) async-start(bf16[8,480,128]{2,1,0:T(8,128)(2,1)} %bitcast.137), calls=%async_computation.2 | async-start | bytes 1966080 | tf_op jit(solution)/shard_map/all_to_all | solution.py:142
  94.2 1.2 convolution_convert_fusion.3
  95.4 1.6 select_bitcast_fusion.1
  97.2 1.6 copy.50
  98.8 2.2 %broadcast_in_dim_reshape.11 = bf16[1,128,2048]{2,1,0:T(8,128)(2,1)} reshape(bf16[128,8,2,128]{3,2,1,0:T(2,128)(2,1)} %copy.50) | data formatting | bytes 1048576 | tf_op jit(solution)/shard_map/broadcast_in_dim;reshape | solution.py:193
  103.0 16.8 %all-to-all-done.2 = bf16[8,480,128]{2,1,0:T(8,128)(2,1)} async-done(((bf16[8,480,128]{2,1,0:T(8,128)(2,1)}), bf16[8,480,128]{2,1,0:T(8,128)(2,1)}, u32[]{:S(2)}, u32[]{:S(2)}) %all-to-all-start.2) | async-done | bytes 983072 | tf_op jit(solution)/shard_map/all_to_all | solution.py:142
  119.9 1.3 reduce_sum.88
  121.9 9.7 %all-to-all-start.3 = ((bf16[32,15,128]{2,1,0:T(8,128)(2,1)}), bf16[32,15,128]{2,1,0:T(8,128)(2,1)S(1)}, u32[]{:S(2)}, u32[]{:S(2)}) async-start(bf16[32,15,128]{2,1,0:T(8,128)(2,1)} %reshape.302), calls=%async_computation.3 | async-start | bytes 262144 | tf_op jit(solution)/shard_map/all_to_all | solution.py:157
  131.7 0.8 copy.48
  132.6 0.8 copy.49
  133.4 7.2 %all-to-all-done.3 = bf16[32,15,128]{2,1,0:T(8,128)(2,1)S(1)} async-done(((bf16[32,15,128]{2,1,0:T(8,128)(2,1)}), bf16[32,15,128]{2,1,0:T(8,128)(2,1)S(1)}, u32[]{:S(2)}, u32[]{:S(2)}) %all-to-all-start.3) | async-done | bytes 122912 | tf_op jit(solution)/shard_map/all_to_all | solution.py:157
  141.0 19.1 %all_gather.7 = bf16[192,2048]{1,0:T(8,128)(2,1)S(1)} all-gather(bf16[192,128]{1,0:T(8,128)(2,1)S(1)} %fusion.6), channel_id=1, replica_groups=mesh['sp'=32,'y'=8,'c'=2] {'y','c'}, dimensions={1}, use_global_device_ids=true | all-gather | bytes 835584 | tf_op jit(solution)/shard_map/all_gather | solution.py:161
  160.9 0.8 broadcast_in_dim.121
  161.7 5.6 %all-to-all-start.5 = ((bf16[32,48,96]{2,1,0:T(8,128)(2,1)}), bf16[32,48,96]{2,1,0:T(8,128)(2,1)S(1)}, u32[]{:S(2)}, u32[]{:S(2)}) async-start(bf16[32,48,96]{2,1,0:T(8,128)(2,1)} %broadcast_in_dim.121), calls=%async_computation.5 | async-start | bytes 786432 | tf_op jit(solution)/shard_map/all_to_all | solution.py:168
  167.7 1.0 copy.52
  169.3 12.9 %all-to-all-done.5 = bf16[32,48,96]{2,1,0:T(8,128)(2,1)S(1)} async-done(((bf16[32,48,96]{2,1,0:T(8,128)(2,1)}), bf16[32,48,96]{2,1,0:T(8,128)(2,1)S(1)}, u32[]{:S(2)}, u32[]{:S(2)}) %all-to-all-start.5) | async-done | bytes 294944 | tf_op jit(solution)/shard_map/all_to_all | solution.py:168
  182.2 5.6 %all-to-all-start.4 = ((bf16[32,64,96]{2,1,0:T(8,128)(2,1)}), bf16[32,64,96]{2,1,0:T(8,128)(2,1)S(1)}, u32[]{:S(2)}, u32[]{:S(2)}) async-start(bf16[32,64,96]{2,1,0:T(8,128)(2,1)} %bitcast.33), calls=%async_computation.4 | async-start | bytes 1048576 | tf_op jit(solution)/shard_map/all_to_all | solution.py:170
  187.8 0.8 fusion.10
  188.8 0.8 fusion.11
  189.6 0.8 fusion.5
  190.4 13.7 %all-to-all-done.4 = bf16[32,64,96]{2,1,0:T(8,128)(2,1)S(1)} async-done(((bf16[32,64,96]{2,1,0:T(8,128)(2,1)}), bf16[32,64,96]{2,1,0:T(8,128)(2,1)S(1)}, u32[]{:S(2)}, u32[]{:S(2)}) %all-to-all-start.4) | async-done | bytes 393248 | tf_op jit(solution)/shard_map/all_to_all | solution.py:170
  204.1 0.7 convert_reduce_fusion
  (82 shorter events, 10.3 us)
Async XLA Ops:
  0.6 159.4 %copy-start = (bf16[96,2048]{1,0:T(8,128)(2,1)S(1)}, bf16[96,2048]{1,0:T(8,128)(2,1)}, u32[]{:S(2)}) copy-start(bf16[96,2048]{1,0:T(8,128)(2,1)} %param.21) | copy-start | bytes 1179652
  0.6 21.4 %copy-start.9 = (bf16[192,2048]{1,0:T(8,128)(2,1)S(1)}, bf16[192,2048]{1,0:T(8,128)(2,1)}, u32[]{:S(2)}) copy-start(bf16[192,2048]{1,0:T(8,128)(2,1)} %param.14) | copy-start | bytes 2359300
  8.6 22.3 %all-to-all-start.1 = ((bf16[32,16,128]{2,1,0:T(8,128)(2,1)}), bf16[32,16,128]{2,1,0:T(8,128)(2,1)S(1)}, u32[]{:S(2)}, u32[]{:S(2)}) async-start(bf16[32,16,128]{2,1,0:T(8,128)(2,1)} %broadcast_select_fusion.4), calls=%async_computation.1 | async-start | bytes 262144 | tf_op jit(solution)/shard_map/all_to_all | solution.py:116
  30.9 5.5 %copy-start.10 = (bf16[32,16,128]{2,1,0:T(8,128)(2,1)}, bf16[32,16,128]{2,1,0:T(8,128)(2,1)S(1)}, u32[]{:S(2)}) copy-start(bf16[32,16,128]{2,1,0:T(8,128)(2,1)S(1)} %all-to-all-done.1) | copy-start | bytes 393220
  30.9 40.4 %all-to-all-start = ((bf16[32,16,1024]{2,1,0:T(8,128)(2,1)}), bf16[32,16,1024]{2,1,0:T(8,128)(2,1)S(1)}, u32[]{:S(2)}, u32[]{:S(2)}) async-start(bf16[32,16,1024]{2,1,0:T(8,128)(2,1)} %bitcast.7), calls=%async_computation | async-start | bytes 2097152 | tf_op jit(solution)/shard_map/all_to_all | solution.py:117
  65.1 10.5 %collective-permute-start = (bf16[480,1024]{1,0:T(8,128)(2,1)S(1)}, bf16[480,1024]{1,0:T(8,128)(2,1)}, u32[]{:S(2)}, u32[]{:S(2)}) collective-permute-start(bf16[480,1024]{1,0:T(8,128)(2,1)S(1)} %all_gather.6), channel_id=1, source_target_pairs={{0,1},{1,0},{2,3},{3,2},{4,5},{5,4},{6,7},{7,6},{8,9},{9,8},{10,11... | collective-permute-start | bytes 2949128 | tf_op jit(solution)/shard_map/ppermute | solution.py:123
  71.6 5.7 %copy-start.3 = (bf16[8,1,128,128]{3,2,1,0:T(8,128)(2,1)S(1)}, bf16[8,1,128,128]{3,2,1,0:T(8,128)(2,1)}, u32[]{:S(2)}) copy-start(bf16[8,1,128,128]{3,2,1,0:T(8,128)(2,1)} %get-tuple-element.20) | copy-start | bytes 786436
  71.7 6.6 %collective-permute-start.1 = (bf16[480,1024]{1,0:T(8,128)(2,1)S(1)}, bf16[480,1024]{1,0:T(8,128)(2,1)S(1)}, u32[]{:S(2)}, u32[]{:S(2)}) collective-permute-start(bf16[480,1024]{1,0:T(8,128)(2,1)S(1)} %reshape.290), channel_id=1, source_target_pairs={{0,1},{1,0},{2,3},{3,2},{4,5},{5,4},{6,7},{7,6},{8,9},{9,8},{10,11... | collective-permute-start | bytes 2949128 | tf_op jit(solution)/shard_map/ppermute | solution.py:122
  75.6 2.2 %copy-start.1 = (bf16[8,1,128,128]{3,2,1,0:T(8,128)(2,1)S(1)}, bf16[8,1,128,128]{3,2,1,0:T(8,128)(2,1)}, u32[]{:S(2)}) copy-start(bf16[8,1,128,128]{3,2,1,0:T(8,128)(2,1)} %get-tuple-element.33) | copy-start | bytes 786436
  75.6 2.6 %copy-start.4 = (bf16[8,1,128,128]{3,2,1,0:T(8,128)(2,1)S(1)}, bf16[8,1,128,128]{3,2,1,0:T(8,128)(2,1)}, u32[]{:S(2)}) copy-start(bf16[8,1,128,128]{3,2,1,0:T(8,128)(2,1)} %get-tuple-element.19) | copy-start | bytes 786436
  77.8 1.0 copy-start.8
  79.8 1.8 copy-start.5
  81.6 5.3 %collective-permute-start.2 = (bf16[480,1024]{1,0:T(8,128)(2,1)}, bf16[480,1024]{1,0:T(8,128)(2,1)}, u32[]{:S(2)}, u32[]{:S(2)}) collective-permute-start(bf16[480,1024]{1,0:T(8,128)(2,1)} %add_convert_fusion.1), channel_id=1, source_target_pairs={{0,1},{1,0},{2,3},{3,2},{4,5},{5,4},{6,7},{7,6},{8,9},{9,8},{10,11... | collective-permute-start | bytes 2949128 | tf_op jit(solution)/shard_map/ppermute | solution.py:138
  83.6 3.4 %copy-start.2 = (bf16[8,1,128,128]{3,2,1,0:T(8,128)(2,1)S(1)}, bf16[8,1,128,128]{3,2,1,0:T(8,128)(2,1)}, u32[]{:S(2)}) copy-start(bf16[8,1,128,128]{3,2,1,0:T(8,128)(2,1)} %get-tuple-element.33) | copy-start | bytes 786436
  83.6 3.4 %copy-start.6 = (bf16[480,128]{1,0:T(8,128)(2,1)S(1)}, bf16[480,128]{1,0:T(8,128)(2,1)}, u32[]{:S(2)}) copy-start(bf16[480,128]{1,0:T(8,128)(2,1)} %copy-done.5) | copy-start | bytes 368644
  89.7 30.1 %all-to-all-start.2 = ((bf16[8,480,128]{2,1,0:T(8,128)(2,1)}), bf16[8,480,128]{2,1,0:T(8,128)(2,1)}, u32[]{:S(2)}, u32[]{:S(2)}) async-start(bf16[8,480,128]{2,1,0:T(8,128)(2,1)} %bitcast.137), calls=%async_computation.2 | async-start | bytes 1966080 | tf_op jit(solution)/shard_map/all_to_all | solution.py:142
  97.2 4.3 %copy-start.7 = (bf16[480,128]{1,0:T(8,128)(2,1)S(1)}, bf16[480,128]{1,0:T(8,128)(2,1)}, u32[]{:S(2)}) copy-start(bf16[480,128]{1,0:T(8,128)(2,1)} %copy-done.5) | copy-start | bytes 368644
  121.9 18.7 %all-to-all-start.3 = ((bf16[32,15,128]{2,1,0:T(8,128)(2,1)}), bf16[32,15,128]{2,1,0:T(8,128)(2,1)S(1)}, u32[]{:S(2)}, u32[]{:S(2)}) async-start(bf16[32,15,128]{2,1,0:T(8,128)(2,1)} %reshape.302), calls=%async_computation.3 | async-start | bytes 262144 | tf_op jit(solution)/shard_map/all_to_all | solution.py:157
  131.7 9.0 %copy-start.16 = (bf16[192,128]{1,0:T(8,128)(2,1)S(1)}, bf16[192,128]{1,0:T(8,128)(2,1)}, u32[]{:S(2)}) copy-start(bf16[192,128]{1,0:T(8,128)(2,1)} %param.15) | copy-start | bytes 147460
  132.6 27.9 %copy-start.13 = (bf16[192,96]{1,0:T(8,128)(2,1)S(1)}, bf16[192,96]{1,0:T(8,128)(2,1)}, u32[]{:S(2)}) copy-start(bf16[192,96]{1,0:T(8,128)(2,1)} %param.22) | copy-start | bytes 110596
  140.7 20.1 %copy-start.11 = (bf16[192,48]{0,1:T(8,128)(2,1)S(1)}, bf16[192,48]{0,1:T(8,128)(2,1)}, u32[]{:S(2)}) copy-start(bf16[192,48]{0,1:T(8,128)(2,1)} %param.23) | copy-start | bytes 55300
  160.1 7.3 %copy-start.14 = (bf16[192,96]{1,0:T(8,128)(2,1)S(1)}, bf16[192,96]{1,0:T(8,128)(2,1)}, u32[]{:S(2)}) copy-start(bf16[192,96]{1,0:T(8,128)(2,1)} %param.25) | copy-start | bytes 110596
  160.5 8.2 %copy-start.12 = (bf16[192,48]{0,1:T(8,128)(2,1)S(1)}, bf16[192,48]{0,1:T(8,128)(2,1)}, u32[]{:S(2)}) copy-start(bf16[192,48]{0,1:T(8,128)(2,1)} %param.24) | copy-start | bytes 55300
  161.7 26.1 %copy-start.15 = (f32[1,1,48,96]{3,2,1,0:T(8,128)S(1)}, f32[1,1,48,96]{3,2,1,0:T(8,128)}, u32[]{:S(2)}) copy-start(f32[1,1,48,96]{3,2,1,0:T(8,128)} %param.27) | copy-start | bytes 55300
  161.7 20.5 %all-to-all-start.5 = ((bf16[32,48,96]{2,1,0:T(8,128)(2,1)}), bf16[32,48,96]{2,1,0:T(8,128)(2,1)S(1)}, u32[]{:S(2)}, u32[]{:S(2)}) async-start(bf16[32,48,96]{2,1,0:T(8,128)(2,1)} %broadcast_in_dim.121), calls=%async_computation.5 | async-start | bytes 786432 | tf_op jit(solution)/shard_map/all_to_all | solution.py:168
  182.2 21.9 %all-to-all-start.4 = ((bf16[32,64,96]{2,1,0:T(8,128)(2,1)}), bf16[32,64,96]{2,1,0:T(8,128)(2,1)S(1)}, u32[]{:S(2)}, u32[]{:S(2)}) async-start(bf16[32,64,96]{2,1,0:T(8,128)(2,1)} %bitcast.33), calls=%async_computation.4 | async-start | bytes 1048576 | tf_op jit(solution)/shard_map/all_to_all | solution.py:170
where the time goes:
time: 206 us; the launch traced here: 205 us
  waiting for transfers between devices  55 us (27%)
  starting transfers between devices  50.6 us (25%)
  blocking collectives  47.7 us (23%)
  matrix products  22.4 us (11%)
  local copies, waits for them, and re-layouts  20 us (10%)
  other arithmetic  6.5 us (3%)
  between operations  2.54 us (1%)
    all_gather x1, blocking collectives, on_device(): grad_own = lax.all_gather(grad_part, 'y', axis=1, tiled=True)  28.7 us
    dot_general x30, matrix products, dot(): return lax.dot_general(a, b, dims, preferred_element_type=F32)  22.4 us
    all_gather x1, blocking collectives, on_device(): stream = lax.all_gather(stream_part, TP, axis=1, tiled=True)  19.1 us
    all_to_all x1, waiting for transfers between devices, on_device(): pieces = lax.all_to_all(pieces, 'y', 0, 0, tiled=True)  16.8 us
    all_to_all x1, waiting for transfers between devices, on_device(): lax.all_to_all(proj_part.reshape(sp_count, width // sp_count, value_dim),...  13.7 us
    all_to_all x1, starting transfers between devices, on_device(): got_grad = lax.all_to_all(send_grad, 'sp', 0, 0, tiled=True)  13.5 us
    all_to_all x1, waiting for transfers between devices, on_device(): states = lax.all_to_all(sent, 'sp', 0, 0, tiled=True)  12.9 us
    all_to_all x1, starting transfers between devices, on_device(): lax.all_to_all(share.reshape(sp_count, capacity, chunk), 'sp', 0, 0, tile...  9.71 us
  transfers between devices with their start and end apart: 9, of which 5 were waited for; matrix products, arithmetic and copies ran while one was open for 15% of the time, Pallas kernels for 0%

commit v1 on v0

--- a/solution.py
+++ b/solution.py
@@ -10,6 +10,13 @@
 ACROSS = (((1,), (1,)), ((), ()))
 ALONG = (((0,), (0,)), ((), ()))
 SWAP = [(0, 1), (1, 0)]
+
+
+def gather_over(x, axis, dim):
+    size = lax.axis_size(axis)
+    pieces = jnp.stack([x for _ in range(size)])
+    pieces = lax.all_to_all(pieces, axis, split_axis=0, concat_axis=0)
+    return jnp.concatenate(pieces, axis=dim)
 
 
 def dot(a, b, dims=(((1,), (0,)), ((), ()))):
@@ -118,7 +125,7 @@
     rows_own = got_rows[:, :capacity].reshape(slot_count, -1)
     grad_part = got_grad[:, :capacity].reshape(slot_count, -1)
     ends = jnp.sum(got_grad[:, capacity, :3].astype(F32), axis=1)
-    grad_own = lax.all_gather(grad_part, "y", axis=1, tiled=True)
+    grad_own = gather_over(grad_part, "y", 1)
     rows_other = lax.ppermute(rows_own, "c", SWAP)
     grad_other = lax.ppermute(grad_own, "c", SWAP)
     gate_own, gate_other = (parity_rows(w_gate[0], k) for k in (core, 1 - core))

time: 206 us -> 229 us (1.11)
  waiting for transfers between devices: 55 us -> 92.8 us
  starting transfers between devices: 50.6 us -> 40.1 us
  blocking collectives: 47.7 us -> 41 us
    all_gather x1 -> x0, blocking collectives: 28.7 us -> none  [on_device(): grad_own = lax.all_gather(grad_part, 'y', axis=1, tiled=True)]
    all_to_all x0 -> x1, blocking collectives: none -> 22.3 us  [on_device(): got_grad = lax.all_to_all(send_grad, 'sp', 0, 0, tiled=True)]
    all_to_all x1, waiting for transfers between devices: 0.01 us -> 20.8 us  [on_device(): got_rows = lax.all_to_all(send_rows, 'sp', 0, 0, tiled=True)]
    all_to_all x1, waiting for transfers between devices: 4.32 us -> 21.4 us  [gather_over(): pieces = lax.all_to_all(pieces, axis, split_axis=0, concat_axis=0)]
    all_to_all x1, starting transfers between devices: 13.5 us -> 7.1 us  [gather_over(): pieces = lax.all_to_all(pieces, axis, split_axis=0, concat_axis=0)]
    all_to_all x1, starting transfers between devices: 9.71 us -> 5.57 us  [on_device(): lax.all_to_all(share.reshape(sp_count, capacity, chunk), 'sp', 0, 0, tile...]
  transfers between devices with their start and end apart: 9 -> 9, of which waited for: 5 -> 6; matrix products, arithmetic and copies ran while one was open for 15% -> 15% of each run, Pallas kernels for 0% -> 0%
where the time goes in v1:
time: 229 us; the launch traced here: 228 us
  waiting for transfers between devices  92.8 us (41%)
  blocking collectives  41 us (18%)
  starting transfers between devices  40.1 us (18%)
  matrix products  23.3 us (10%)
  local copies, waits for them, and re-layouts  22.2 us (10%)
  other arithmetic  5.85 us (3%)
  between operations  2.53 us (1%)
    dot_general x30, matrix products, dot(): return lax.dot_general(a, b, dims, preferred_element_type=F32)  23.3 us
    all_to_all x1, blocking collectives, on_device(): got_grad = lax.all_to_all(send_grad, 'sp', 0, 0, tiled=True)  22.3 us
    all_to_all x1, waiting for transfers between devices, gather_over(): pieces = lax.all_to_all(pieces, axis, split_axis=0, concat_axis=0)  21.4 us
    all_to_all x1, waiting for transfers between devices, on_device(): got_rows = lax.all_to_all(send_rows, 'sp', 0, 0, tiled=True)  20.8 us
    all_gather x1, blocking collectives, on_device(): stream = lax.all_gather(stream_part, TP, axis=1, tiled=True)  18.7 us
    all_to_all x1, waiting for transfers between devices, on_device(): pieces = lax.all_to_all(pieces, 'y', 0, 0, tiled=True)  16.8 us
    all_to_all x1, waiting for transfers between devices, on_device(): lax.all_to_all(proj_part.reshape(sp_count, width // sp_count, value_dim),...  13.7 us
    all_to_all x1, waiting for transfers between devices, on_device(): states = lax.all_to_all(sent, 'sp', 0, 0, tiled=True)  12.9 us
  transfers between devices with their start and end apart: 9, of which 6 were waited for; matrix products, arithmetic and copies ran while one was open for 15% of the time, Pallas kernels for 0%

profile of v1, /device:TPU:2, one launch (start us, length us, event | category | flops | bytes accessed | tf_op | source)
XLA Modules:
  0.0 227.8 jit_solution(4255302092431208316)
XLA Ops:
  3.9 0.8 fusion.41
  4.9 0.8 fusion.40
  6.6 1.2 fusion.1
  7.9 22.3 %all_to_all.35 = bf16[32,16,128]{2,1,0:T(8,128)(2,1)S(1)} all-to-all(bf16[32,16,128]{2,1,0:T(8,128)(2,1)S(1)} %broadcast_select_fusion.4), channel_id=1, replica_groups=mesh['sp'=32,'y'=8,'c'=2] {'sp'}, dimensions={0} | all-to-all | bytes 262144 | tf_op jit(solution)/shard_map/all_to_all | solution.py:123
  30.2 1.1 stack.3
  31.3 7.1 %all-to-all-start.2 = ((bf16[8,480,128]{2,1,0:T(8,128)(2,1)}), bf16[8,480,128]{2,1,0:T(8,128)(2,1)S(1)}, u32[]{:S(2)}, u32[]{:S(2)}) async-start(bf16[8,480,128]{2,1,0:T(8,128)(2,1)} %stack.3), calls=%async_computation.2 | async-start | bytes 1966080 | tf_op jit(solution)/shard_map/all_to_all | solution.py:18
  39.0 2.3 %dynamic-slice_reduce_fusion = bf16[192,8,128]{2,1,0:T(8,128)(2,1)S(1)} fusion(bf16[192,8,2,128]{3,2,1,0:T(2,128)(2,1)S(1)} %reshape.292, s32[]{:T(128)S(6)} %select_n.175), kind=kLoop, calls=%fused_computation.38 | loop fusion | bytes 786436 | tf_op jit(solution)/shard_map/jit(dynamic_index_in_dim)/dynamic_slice | solution.py:49
  41.4 1.6 convolution_convert_fusion.1
  42.9 21.4 %all-to-all-done.2 = bf16[8,480,128]{2,1,0:T(8,128)(2,1)S(1)} async-done(((bf16[8,480,128]{2,1,0:T(8,128)(2,1)}), bf16[8,480,128]{2,1,0:T(8,128)(2,1)S(1)}, u32[]{:S(2)}, u32[]{:S(2)}) %all-to-all-start.2) | async-done | bytes 983072 | tf_op jit(solution)/shard_map/all_to_all | solution.py:18
  64.3 5.4 %all-to-all-start = ((bf16[32,16,1024]{2,1,0:T(8,128)(2,1)}), bf16[32,16,1024]{2,1,0:T(8,128)(2,1)S(1)}, u32[]{:S(2)}, u32[]{:S(2)}) async-start(bf16[32,16,1024]{2,1,0:T(8,128)(2,1)} %bitcast.157), calls=%async_computation | async-start | bytes 2097152 | tf_op jit(solution)/shard_map/all_to_all | solution.py:124
  69.8 1.3 copy.49
  71.1 1.1 copy_bitcast_fusion
  72.2 1.9 collective-permute-start
  74.1 0.9 constant_dynamic-slice_fusion.4
  75.0 2.2 constant_dynamic-slice_fusion
  77.2 20.8 %all-to-all-done = bf16[32,16,1024]{2,1,0:T(8,128)(2,1)S(1)} async-done(((bf16[32,16,1024]{2,1,0:T(8,128)(2,1)}), bf16[32,16,1024]{2,1,0:T(8,128)(2,1)S(1)}, u32[]{:S(2)}, u32[]{:S(2)}) %all-to-all-start) | async-done | bytes 1048608 | tf_op jit(solution)/shard_map/all_to_all | solution.py:124
  98.3 2.1 collective-permute-start.1
  100.4 1.4 fusion.38
  101.8 1.4 fusion.45
  103.6 1.7 convolution_add_fusion.2
  105.8 1.1 multiply_convert_fusion
  107.3 1.4 add_convert_fusion.1
  108.7 2.4 %collective-permute-start.2 = (bf16[480,1024]{1,0:T(8,128)(2,1)}, bf16[480,1024]{1,0:T(8,128)(2,1)}, u32[]{:S(2)}, u32[]{:S(2)}) collective-permute-start(bf16[480,1024]{1,0:T(8,128)(2,1)} %add_convert_fusion.1), channel_id=1, source_target_pairs={{0,1},{1,0},{2,3},{3,2},{4,5},{5,4},{6,7},{7,6},{8,9},{9,8},{10,11... | collective-permute-start | bytes 2949128 | tf_op jit(solution)/shard_map/ppermute | solution.py:145
  111.8 1.2 fusion.27
  113.1 1.4 fusion.46
  114.5 1.6 fusion
  116.2 1.1 copy.71
  117.3 4.4 %all-to-all-start.3 = ((bf16[8,480,128]{2,1,0:T(8,128)(2,1)}), bf16[8,480,128]{2,1,0:T(8,128)(2,1)}, u32[]{:S(2)}, u32[]{:S(2)}) async-start(bf16[8,480,128]{2,1,0:T(8,128)(2,1)} %bitcast.149), calls=%async_computation.3 | async-start | bytes 1966080 | tf_op jit(solution)/shard_map/all_to_all | solution.py:149
  121.7 1.2 convolution_convert_fusion.3
  123.0 1.6 select_bitcast_fusion.1
  124.8 1.6 copy.52
  126.4 2.2 broadcast_in_dim_reshape.11
  130.6 16.8 %all-to-all-done.3 = bf16[8,480,128]{2,1,0:T(8,128)(2,1)} async-done(((bf16[8,480,128]{2,1,0:T(8,128)(2,1)}), bf16[8,480,128]{2,1,0:T(8,128)(2,1)}, u32[]{:S(2)}, u32[]{:S(2)}) %all-to-all-start.3) | async-done | bytes 983072 | tf_op jit(solution)/shard_map/all_to_all | solution.py:149
  147.4 1.3 reduce_sum.88
  149.4 5.6 %all-to-all-start.4 = ((bf16[32,15,128]{2,1,0:T(8,128)(2,1)}), bf16[32,15,128]{2,1,0:T(8,128)(2,1)S(1)}, u32[]{:S(2)}, u32[]{:S(2)}) async-start(bf16[32,15,128]{2,1,0:T(8,128)(2,1)} %reshape.308), calls=%async_computation.4 | async-start | bytes 262144 | tf_op jit(solution)/shard_map/all_to_all | solution.py:164
  155.0 0.8 copy.50
  155.9 0.8 copy.51
  156.8 7.1 %all-to-all-done.4 = bf16[32,15,128]{2,1,0:T(8,128)(2,1)S(1)} async-done(((bf16[32,15,128]{2,1,0:T(8,128)(2,1)}), bf16[32,15,128]{2,1,0:T(8,128)(2,1)S(1)}, u32[]{:S(2)}, u32[]{:S(2)}) %all-to-all-start.4) | async-done | bytes 122912 | tf_op jit(solution)/shard_map/all_to_all | solution.py:164
  164.2 18.7 %all_gather.3 = bf16[192,2048]{1,0:T(8,128)(2,1)S(1)} all-gather(bf16[192,128]{1,0:T(8,128)(2,1)S(1)} %fusion.6), channel_id=1, replica_groups=mesh['sp'=32,'y'=8,'c'=2] {'y','c'}, dimensions={1}, use_global_device_ids=true | all-gather | bytes 835584 | tf_op jit(solution)/shard_map/all_gather | solution.py:168
  183.8 0.8 broadcast_in_dim.121
  184.6 5.6 %all-to-all-start.6 = ((bf16[32,48,96]{2,1,0:T(8,128)(2,1)}), bf16[32,48,96]{2,1,0:T(8,128)(2,1)S(1)}, u32[]{:S(2)}, u32[]{:S(2)}) async-start(bf16[32,48,96]{2,1,0:T(8,128)(2,1)} %broadcast_in_dim.121), calls=%async_computation.6 | async-start | bytes 786432 | tf_op jit(solution)/shard_map/all_to_all | solution.py:175
  190.6 1.0 copy.54
  192.2 12.9 %all-to-all-done.6 = bf16[32,48,96]{2,1,0:T(8,128)(2,1)S(1)} async-done(((bf16[32,48,96]{2,1,0:T(8,128)(2,1)}), bf16[32,48,96]{2,1,0:T(8,128)(2,1)S(1)}, u32[]{:S(2)}, u32[]{:S(2)}) %all-to-all-start.6) | async-done | bytes 294944 | tf_op jit(solution)/shard_map/all_to_all | solution.py:175
  205.1 5.6 %all-to-all-start.5 = ((bf16[32,64,96]{2,1,0:T(8,128)(2,1)}), bf16[32,64,96]{2,1,0:T(8,128)(2,1)S(1)}, u32[]{:S(2)}, u32[]{:S(2)}) async-start(bf16[32,64,96]{2,1,0:T(8,128)(2,1)} %bitcast.34), calls=%async_computation.5 | async-start | bytes 1048576 | tf_op jit(solution)/shard_map/all_to_all | solution.py:177
  210.7 0.8 fusion.10
  211.7 0.8 fusion.11
  212.5 0.8 fusion.5
  213.3 13.7 %all-to-all-done.5 = bf16[32,64,96]{2,1,0:T(8,128)(2,1)S(1)} async-done(((bf16[32,64,96]{2,1,0:T(8,128)(2,1)}), bf16[32,64,96]{2,1,0:T(8,128)(2,1)S(1)}, u32[]{:S(2)}, u32[]{:S(2)}) %all-to-all-start.5) | async-done | bytes 393248 | tf_op jit(solution)/shard_map/all_to_all | solution.py:177
  (84 shorter events, 12.1 us)
Async XLA Ops:
  0.6 182.3 %copy-start = (bf16[96,2048]{1,0:T(8,128)(2,1)S(1)}, bf16[96,2048]{1,0:T(8,128)(2,1)}, u32[]{:S(2)}) copy-start(bf16[96,2048]{1,0:T(8,128)(2,1)} %param.21) | copy-start | bytes 1179652
  7.8 30.7 %copy-start.9 = (bf16[192,2048]{1,0:T(8,128)(2,1)S(1)}, bf16[192,2048]{1,0:T(8,128)(2,1)}, u32[]{:S(2)}) copy-start(bf16[192,2048]{1,0:T(8,128)(2,1)} %param.14) | copy-start | bytes 2359300
  30.1 8.3 %copy-start.10 = (bf16[32,16,128]{2,1,0:T(8,128)(2,1)}, bf16[32,16,128]{2,1,0:T(8,128)(2,1)S(1)}, u32[]{:S(2)}) copy-start(bf16[32,16,128]{2,1,0:T(8,128)(2,1)S(1)} %all_to_all.35) | copy-start | bytes 393220
  31.3 33.0 %all-to-all-start.2 = ((bf16[8,480,128]{2,1,0:T(8,128)(2,1)}), bf16[8,480,128]{2,1,0:T(8,128)(2,1)S(1)}, u32[]{:S(2)}, u32[]{:S(2)}) async-start(bf16[8,480,128]{2,1,0:T(8,128)(2,1)} %stack.3), calls=%async_computation.2 | async-start | bytes 1966080 | tf_op jit(solution)/shard_map/all_to_all | solution.py:18
  64.3 33.7 %all-to-all-start = ((bf16[32,16,1024]{2,1,0:T(8,128)(2,1)}), bf16[32,16,1024]{2,1,0:T(8,128)(2,1)S(1)}, u32[]{:S(2)}, u32[]{:S(2)}) async-start(bf16[32,16,1024]{2,1,0:T(8,128)(2,1)} %bitcast.157), calls=%async_computation | async-start | bytes 2097152 | tf_op jit(solution)/shard_map/all_to_all | solution.py:124
  72.2 31.4 %collective-permute-start = (bf16[480,1024]{1,0:T(8,128)(2,1)}, bf16[480,1024]{1,0:T(8,128)(2,1)}, u32[]{:S(2)}, u32[]{:S(2)}) collective-permute-start(bf16[480,1024]{1,0:T(8,128)(2,1)} %copy_bitcast_fusion), channel_id=1, source_target_pairs={{0,1},{1,0},{2,3},{3,2},{4,5},{5,4},{6,7},{7,6},{8,9},{9,8},{10,11... | collective-permute-start | bytes 2949128 | tf_op jit(solution)/shard_map/ppermute | solution.py:130
  98.3 4.9 %copy-start.1 = (bf16[8,1,128,128]{3,2,1,0:T(8,128)(2,1)S(1)}, bf16[8,1,128,128]{3,2,1,0:T(8,128)(2,1)}, u32[]{:S(2)}) copy-start(bf16[8,1,128,128]{3,2,1,0:T(8,128)(2,1)} %get-tuple-element.33) | copy-start | bytes 786436
  98.3 7.0 %collective-permute-start.1 = (bf16[480,1024]{1,0:T(8,128)(2,1)S(1)}, bf16[480,1024]{1,0:T(8,128)(2,1)S(1)}, u32[]{:S(2)}, u32[]{:S(2)}) collective-permute-start(bf16[480,1024]{1,0:T(8,128)(2,1)S(1)} %reshape.295), channel_id=1, source_target_pairs={{0,1},{1,0},{2,3},{3,2},{4,5},{5,4},{6,7},{7,6},{8,9},{9,8},{10,11... | collective-permute-start | bytes 2949128 | tf_op jit(solution)/shard_map/ppermute | solution.py:129
  100.4 3.3 %copy-start.7 = (bf16[128,8,1,128]{0,3,2,1:T(8,128)(2,1)S(1)}, bf16[128,8,1,128]{0,3,2,1:T(8,128)(2,1)}, u32[]{:S(2)}) copy-start(bf16[128,8,1,128]{0,3,2,1:T(8,128)(2,1)} %get-tuple-element.17) | copy-start | bytes 786436
  103.2 2.2 copy-start.3
  103.6 2.2 copy-start.8
  106.9 1.8 copy-start.4
  108.7 5.8 %collective-permute-start.2 = (bf16[480,1024]{1,0:T(8,128)(2,1)}, bf16[480,1024]{1,0:T(8,128)(2,1)}, u32[]{:S(2)}, u32[]{:S(2)}) collective-permute-start(bf16[480,1024]{1,0:T(8,128)(2,1)} %add_convert_fusion.1), channel_id=1, source_target_pairs={{0,1},{1,0},{2,3},{3,2},{4,5},{5,4},{6,7},{7,6},{8,9},{9,8},{10,11... | collective-permute-start | bytes 2949128 | tf_op jit(solution)/shard_map/ppermute | solution.py:145
  111.1 3.4 %copy-start.2 = (bf16[8,1,128,128]{3,2,1,0:T(8,128)(2,1)S(1)}, bf16[8,1,128,128]{3,2,1,0:T(8,128)(2,1)}, u32[]{:S(2)}) copy-start(bf16[8,1,128,128]{3,2,1,0:T(8,128)(2,1)} %get-tuple-element.33) | copy-start | bytes 786436
  111.1 3.4 %copy-start.5 = (bf16[480,128]{1,0:T(8,128)(2,1)S(1)}, bf16[480,128]{1,0:T(8,128)(2,1)}, u32[]{:S(2)}) copy-start(bf16[480,128]{1,0:T(8,128)(2,1)} %copy-done.4) | copy-start | bytes 368644
  117.3 30.1 %all-to-all-start.3 = ((bf16[8,480,128]{2,1,0:T(8,128)(2,1)}), bf16[8,480,128]{2,1,0:T(8,128)(2,1)}, u32[]{:S(2)}, u32[]{:S(2)}) async-start(bf16[8,480,128]{2,1,0:T(8,128)(2,1)} %bitcast.149), calls=%async_computation.3 | async-start | bytes 1966080 | tf_op jit(solution)/shard_map/all_to_all | solution.py:149
  124.7 4.3 %copy-start.6 = (bf16[480,128]{1,0:T(8,128)(2,1)S(1)}, bf16[480,128]{1,0:T(8,128)(2,1)}, u32[]{:S(2)}) copy-start(bf16[480,128]{1,0:T(8,128)(2,1)} %copy-done.4) | copy-start | bytes 368644
  149.4 14.5 %all-to-all-start.4 = ((bf16[32,15,128]{2,1,0:T(8,128)(2,1)}), bf16[32,15,128]{2,1,0:T(8,128)(2,1)S(1)}, u32[]{:S(2)}, u32[]{:S(2)}) async-start(bf16[32,15,128]{2,1,0:T(8,128)(2,1)} %reshape.308), calls=%async_computation.4 | async-start | bytes 262144 | tf_op jit(solution)/shard_map/all_to_all | solution.py:164
  155.0 8.9 %copy-start.16 = (bf16[192,128]{1,0:T(8,128)(2,1)S(1)}, bf16[192,128]{1,0:T(8,128)(2,1)}, u32[]{:S(2)}) copy-start(bf16[192,128]{1,0:T(8,128)(2,1)} %param.15) | copy-start | bytes 147460
  155.9 27.4 %copy-start.13 = (bf16[192,96]{1,0:T(8,128)(2,1)S(1)}, bf16[192,96]{1,0:T(8,128)(2,1)}, u32[]{:S(2)}) copy-start(bf16[192,96]{1,0:T(8,128)(2,1)} %param.22) | copy-start | bytes 110596
  163.9 19.7 %copy-start.11 = (bf16[192,48]{0,1:T(8,128)(2,1)S(1)}, bf16[192,48]{0,1:T(8,128)(2,1)}, u32[]{:S(2)}) copy-start(bf16[192,48]{0,1:T(8,128)(2,1)} %param.23) | copy-start | bytes 55300
  182.9 7.3 %copy-start.14 = (bf16[192,96]{1,0:T(8,128)(2,1)S(1)}, bf16[192,96]{1,0:T(8,128)(2,1)}, u32[]{:S(2)}) copy-start(bf16[192,96]{1,0:T(8,128)(2,1)} %param.25) | copy-start | bytes 110596
  183.3 8.3 %copy-start.12 = (bf16[192,48]{0,1:T(8,128)(2,1)S(1)}, bf16[192,48]{0,1:T(8,128)(2,1)}, u32[]{:S(2)}) copy-start(bf16[192,48]{0,1:T(8,128)(2,1)} %param.24) | copy-start | bytes 55300
  184.6 26.1 %copy-start.15 = (f32[1,1,48,96]{3,2,1,0:T(8,128)S(1)}, f32[1,1,48,96]{3,2,1,0:T(8,128)}, u32[]{:S(2)}) copy-start(f32[1,1,48,96]{3,2,1,0:T(8,128)} %param.27) | copy-start | bytes 55300
  184.6 20.5 %all-to-all-start.6 = ((bf16[32,48,96]{2,1,0:T(8,128)(2,1)}), bf16[32,48,96]{2,1,0:T(8,128)(2,1)S(1)}, u32[]{:S(2)}, u32[]{:S(2)}) async-start(bf16[32,48,96]{2,1,0:T(8,128)(2,1)} %broadcast_in_dim.121), calls=%async_computation.6 | async-start | bytes 786432 | tf_op jit(solution)/shard_map/all_to_all | solution.py:175
  205.1 21.9 %all-to-all-start.5 = ((bf16[32,64,96]{2,1,0:T(8,128)(2,1)}), bf16[32,64,96]{2,1,0:T(8,128)(2,1)S(1)}, u32[]{:S(2)}, u32[]{:S(2)}) async-start(bf16[32,64,96]{2,1,0:T(8,128)(2,1)} %bitcast.34), calls=%async_computation.5 | async-start | bytes 1048576 | tf_op jit(solution)/shard_map/all_to_all | solution.py:177
